TPU v7x, 32 devices: a whole 2x2x4 slice. The times are simulated.
32 devices in a mesh: sp: 8 (over z, x), tp: 4 (over y, core).
Axes of the slice: x: 2, y: 2, z: 4, core: 2. Of those that a mesh axis runs over, the one named last changes fastest.
Arguments:
- residual: bfloat16 [4096, 2048], P(('sp', 'tp')), may hold values from -6 to 6
- query_small: bfloat16 [4096, 8, 128], P('sp', 'tp'), may hold values from -120 to 120
- key_small: bfloat16 [4096, 8, 128], P('sp', 'tp'), may hold values from -6 to 6
- value_small: bfloat16 [4096, 8, 128], P('sp', 'tp'), may hold values from -6 to 6
- query_large: bfloat16 [4096, 8, 256], P('sp', 'tp'), may hold values from -120 to 120
- key_large: bfloat16 [4096, 8, 256], P('sp', 'tp'), may hold values from -6 to 6
- value_large: bfloat16 [4096, 8, 128], P('sp', 'tp'), may hold values from -6 to 6
- lambda_small: float32 [8], P('tp'), may hold values from 0.3 to 0.8
- lambda_large: float32 [8], P('tp'), may hold values from 0.3 to 0.8
- head_gain: float32 [128], replicated, may hold values from 0.1 to 1.9
- output_small: bfloat16 [1024, 2048], P('tp'), may hold values from -0.125 to 0.125
- output_large: bfloat16 [1024, 2048], P('tp'), may hold values from -0.125 to 0.125
- norm_gain: float32 [2048], replicated, may hold values from 0.1 to 1.9
- gate_weight: bfloat16 [2048, 5632], P('sp', 'tp'), may hold values from -0.125 to 0.125
- up_weight: bfloat16 [2048, 5632], P('sp', 'tp'), may hold values from -0.125 to 0.125
- down_weight: bfloat16 [5632, 2048], P('tp', 'sp'), may hold values from -0.3125 to 0.3125
Outputs:
- block_output: bfloat16 [4096, 2048], P(('sp', 'tp'))
All inputs are finite; a program needn't handle non-finite values.
Results may differ from a plain program's by a relative error of at most 0.015.
Values may be sent and summed in bfloat16 or wider, within the bound.
No kernel may reach another device: no remote copies, remote signals or barrier semaphores. Data moves between devices by JAX's collectives and lax.ppermute only.
A program may use at most 128 MiB of HBM per device.

v0:
```python
import math
import jax
import jax.numpy as jnp
from jax import lax
from jax.sharding import PartitionSpec as P

residual_scale = 8.0**0.25
branch_scale = 0.8
norm_epsilon = 1e-05
masked_score = -1e30


def from_partner(value, axis, distance):
    mask = 2**distance
    pairs = [(source, source ^ mask) for source in range(lax.axis_size(axis))]
    return lax.ppermute(value, axis, pairs)


def layer_norm(values, gains):
    centered = values - jnp.mean(values, axis=-1, keepdims=True)
    variance = jnp.mean(centered * centered, axis=-1, keepdims=True)
    return centered * lax.rsqrt(variance + norm_epsilon) * gains


def empty_state(head_count, tokens, width):
    return (
        jnp.full((head_count, 2, tokens), masked_score, jnp.float32),
        jnp.zeros((head_count, 2, tokens), jnp.float32),
        jnp.zeros((head_count, 2, tokens, width), jnp.float32),
    )


def absorb_group(state, query_maps, key_block, value_block, key_index, query_index):
    running_max, totals, accumulated = state
    head_size = query_maps.shape[3]
    scores = jnp.einsum(
        "qhmd,khmd->hmqk", query_maps, key_block, preferred_element_type=jnp.float32
    ) * head_size ** (-0.5)
    visible = key_index[None, :] <= query_index[:, None]
    scores = jnp.where(visible, scores, masked_score)
    new_max = jnp.maximum(running_max, jnp.max(scores, axis=-1))
    fading = jnp.exp(running_max - new_max)
    weights = jnp.where(visible, jnp.exp(scores - new_max[..., None]), 0.0)
    totals = totals * fading + jnp.sum(weights, axis=-1)
    accumulated = accumulated * fading[..., None] + jnp.einsum(
        "hmqk,khe->hmqe",
        weights.astype(jnp.bfloat16),
        value_block,
        preferred_element_type=jnp.float32,
    )
    return (new_max, totals, accumulated)


def finish_group(state, lambdas, head_gain):
    running_max, totals, accumulated = state
    map_out = accumulated / totals[..., None]
    combined = map_out[:, 0] - lambdas[:, None, None] * map_out[:, 1]
    mean_square = jnp.mean(combined * combined, axis=-1, keepdims=True)
    normed = (combined * lax.rsqrt(mean_square + norm_epsilon) * head_gain * branch_scale).astype(
        jnp.bfloat16
    )
    head_count, tokens, width = normed.shape
    return jnp.transpose(normed, (1, 0, 2)).reshape(tokens, head_count * width)


def per_device(
    residual,
    query_small,
    key_small,
    value_small,
    query_large,
    key_large,
    value_large,
    lambda_small,
    lambda_large,
    head_gain,
    output_small,
    output_large,
    norm_gain,
    gate_weight,
    up_weight,
    down_weight,
):
    tokens = query_small.shape[0]
    half = tokens // 2
    own_rows = residual.shape[0]
    bit_count = lax.axis_size("sp").bit_length() - 1
    residual_all = lax.all_gather(residual, "tp", axis=0, tiled=True)
    heads_small = query_small.shape[1]
    heads_large = query_large.shape[1]
    value_width = value_small.shape[2]
    first_start = lax.axis_index("sp") * tokens
    later_small = query_small[half:]
    later_large = query_large[half:]
    for bit in range(bit_count):
        later_small, later_large = from_partner((later_small, later_large), "sp", bit)
    second_start = (lax.axis_size("sp") - 1 - lax.axis_index("sp")) * tokens + half
    halves = (
        (
            query_small[:half].reshape(half, heads_small, 2, -1),
            query_large[:half].reshape(half, heads_large, 2, -1),
            first_start + jnp.arange(half, dtype=jnp.int32),
        ),
        (
            later_small.reshape(half, heads_small, 2, -1),
            later_large.reshape(half, heads_large, 2, -1),
            second_start + jnp.arange(half, dtype=jnp.int32),
        ),
    )
    one_half = (
        empty_state(heads_small, half, value_width),
        empty_state(heads_large, half, value_width),
    )
    keys_first = lax.all_gather(key_small, "sp", axis=0, tiled=True)
    keys_second = lax.all_gather(key_large, "sp", axis=0, tiled=True)
    values_first = lax.all_gather(value_small, "sp", axis=0, tiled=True)
    values_second = lax.all_gather(value_large, "sp", axis=0, tiled=True)
    row_count = keys_first.shape[0]
    block_size = math.gcd(row_count, 512)
    number = row_count // block_size
    stacked = (
        keys_first.reshape(number, block_size, heads_small, 2, -1),
        keys_second.reshape(number, block_size, heads_large, 2, -1),
        values_first.reshape(number, block_size, heads_small, value_width),
        values_second.reshape(number, block_size, heads_large, value_width),
    )

    def step(carried, block_items):
        block_index, blocks = block_items
        key_index = block_index * block_size + jnp.arange(block_size, dtype=jnp.int32)
        updated = []
        for which in range(2):
            maps_small, maps_large, query_index = halves[which]

            def take(pair):
                return (
                    absorb_group(pair[0], maps_small, blocks[0], blocks[2], key_index, query_index),
                    absorb_group(pair[1], maps_large, blocks[1], blocks[3], key_index, query_index),
                )

            def leave(pair):
                return pair

            updated.append(
                lax.cond(key_index[0] <= query_index[half - 1], take, leave, carried[which])
            )
        return ((updated[0], updated[1]), None)

    result, unused = lax.scan(
        step, (one_half, one_half), (jnp.arange(number, dtype=jnp.int32), stacked)
    )
    first_states, second_states = result
    early_small = finish_group(first_states[0], lambda_small, head_gain)
    early_large = finish_group(first_states[1], lambda_large, head_gain)
    late_small = finish_group(second_states[0], lambda_small, head_gain)
    late_large = finish_group(second_states[1], lambda_large, head_gain)
    for bit in range(bit_count):
        late_small, late_large = from_partner((late_small, late_large), "sp", bit)
    attended_small = jnp.concatenate([early_small, late_small], axis=0)
    attended_large = jnp.concatenate([early_large, late_large], axis=0)
    mixed_sum = lax.psum(
        (
            jnp.dot(attended_small, output_small, preferred_element_type=jnp.float32)
            + jnp.dot(attended_large, output_large, preferred_element_type=jnp.float32)
        ).astype(jnp.bfloat16),
        "tp",
    ).astype(jnp.float32)
    whole_rows = layer_norm(
        residual_scale * residual_all.astype(jnp.float32) + mixed_sum, norm_gain
    ).astype(jnp.bfloat16)
    normed = lax.dynamic_slice_in_dim(whole_rows, lax.axis_index("tp") * own_rows, own_rows, 0)
    gate_rows = jnp.dot(
        whole_rows,
        lax.all_gather(gate_weight, "sp", axis=0, tiled=True),
        preferred_element_type=jnp.float32,
    )
    up_rows = jnp.dot(
        whole_rows,
        lax.all_gather(up_weight, "sp", axis=0, tiled=True),
        preferred_element_type=jnp.float32,
    )
    down_full = lax.all_gather(down_weight, "sp", axis=1, tiled=True)
    hidden = (jax.nn.silu(gate_rows) * up_rows).astype(jnp.bfloat16)
    down_sum = lax.psum_scatter(
        jnp.dot(hidden, down_full, preferred_element_type=jnp.float32).astype(jnp.bfloat16),
        "tp",
        scatter_dimension=0,
        tiled=True,
    ).astype(jnp.float32)
    return (residual_scale * normed.astype(jnp.float32) + 0.5 * down_sum).astype(jnp.bfloat16)


def solution(mesh):
    in_specs = (
        P(("sp", "tp"), None),
        P("sp", "tp", None),
        P("sp", "tp", None),
        P("sp", "tp", None),
        P("sp", "tp", None),
        P("sp", "tp", None),
        P("sp", "tp", None),
        P("tp"),
        P("tp"),
        P(),
        P("tp", None),
        P("tp", None),
        P(),
        P("sp", "tp"),
        P("sp", "tp"),
        P("tp", "sp"),
    )
    out_specs = P(("sp", "tp"), None)
    return jax.shard_map(
        per_device, mesh=mesh, in_specs=in_specs, out_specs=out_specs, check_vma=False
    )
```

profile of v0, /device:TPU:0, one launch (start us, length us, event | category | flops | bytes accessed | tf_op | source)
XLA Modules:
  0.0 791.7 jit_solution(11565010698791997182)
XLA Ops:
  15.2 6.3 collective-permute-done.3
  30.0 7.0 collective-permute-done.4
  43.6 29.2 %collective-permute-done.2 = bf16[256,2,128]{2,1,0:T(2,128)(2,1)S(1)} collective-permute-done((bf16[256,2,128]{2,1,0:T(2,128)(2,1)S(1)}, bf16[256,2,128]{2,1,0:T(2,128)(2,1)S(1)}, u32[]{:S(2)}, u32[]{:S(2)}) %collective-permute-start.2) | collective-permute-done | bytes 131104 | tf_op jit(solution)/shard_map/ppermute | solution.py:16
  73.8 9.7 %reshape.126 = bf16[8,512,2,2,64]{4,3,2,1,0:T(2,128)(2,1)} reshape(bf16[4096,2,128]{2,1,0:T(2,128)(2,1)} %all-gather.11.cloned.1.call-done) | data formatting | bytes 4194304 | tf_op jit(solution)/shard_map/reshape | solution.py:122
  83.5 10.6 %copy.56 = bf16[8,512,2,2,64]{1,4,3,2,0:T(8,128)(2,1)} copy(bf16[8,512,2,2,64]{4,3,2,1,0:T(2,128)(2,1)} %reshape.126) | data formatting | bytes 4194304 | tf_op jit(solution)/shard_map/while | solution.py:149
  94.1 54.6 %all-gather.15.cloned.1.call-done = bf16[4096,2,256]{2,1,0:T(2,128)(2,1)} async-done(((bf16[512,2,256]{2,1,0:T(2,128)(2,1)}), bf16[4096,2,256]{2,1,0:T(2,128)(2,1)}) %all-gather.15.cloned.1.call-update) | async-done | bytes 4194320 | tf_op jit(solution)/shard_map/all_gather | solution.py:115
  148.7 11.7 %reshape.127 = bf16[8,512,2,2,128]{4,3,2,1,0:T(2,128)(2,1)} reshape(bf16[4096,2,256]{2,1,0:T(2,128)(2,1)} %all-gather.15.cloned.1.call-done) | data formatting | bytes 8388608 | tf_op jit(solution)/shard_map/reshape | solution.py:123
  160.4 38.1 %all-gather.13.cloned.1.call-done = bf16[4096,2,128]{2,0,1:T(8,128)(2,1)} async-done(((bf16[512,2,128]{2,0,1:T(8,128)(2,1)}), bf16[4096,2,128]{2,0,1:T(8,128)(2,1)}) %all-gather.13.cloned.1.call-update) | async-done | bytes 2097168 | tf_op jit(solution)/shard_map/all_gather | solution.py:116
  198.5 49.7 %all-gather.17.cloned.1.call-done = bf16[4096,2,128]{2,0,1:T(8,128)(2,1)} async-done(((bf16[512,2,128]{2,0,1:T(8,128)(2,1)}), bf16[4096,2,128]{2,0,1:T(8,128)(2,1)}) %all-gather.17.cloned.1.call-update) | async-done | bytes 2097168 | tf_op jit(solution)/shard_map/all_gather | solution.py:117
  251.6 124.7 %while.32 = (s32[]{:T(128)}, f32[2,2,256]{2,1,0:T(2,128)S(1)}, f32[2,2,256]{2,1,0:T(2,128)S(1)}, f32[2,2,256,128]{3,2,1,0:T(8,128)}, f32[2,2,256]{2,1,0:T(2,128)...) while((s32[]{:T(128)}, f32[2,2,256]{2,1,0:T(2,128)S(1)}, ...), condition=%wide.region_13.14_spmd, body=%wide.region_0.13_spmd.sunk | while | flops 968106496 | bytes 58991568 | solution.py:149
  258.8 5.7 conditional.5
  266.5 5.8 conditional.4
  279.4 5.7 conditional.5
  309.1 5.7 conditional.5
  323.9 5.7 conditional.5
  338.8 5.7 conditional.5
  353.6 5.7 conditional.5
  410.6 48.7 %all-reduce.2.cloned.1.call-done = bf16[512,2048]{1,0:T(8,128)(2,1)} async-done(((bf16[512,2048]{1,0:T(8,128)(2,1)}), bf16[512,2048]{1,0:T(8,128)(2,1)}) %all-reduce.2.cloned.1.call-update) | async-done | bytes 2097168 | tf_op jit(solution)/shard_map/psum | solution.py:161
  465.9 88.0 %all-gather.19.cloned.1.call-done = bf16[2048,1408]{1,0:T(8,128)(2,1)} async-done(((bf16[256,1408]{1,0:T(8,128)(2,1)}), bf16[2048,1408]{1,0:T(8,128)(2,1)}) %all-gather.19.cloned.1.call-update) | async-done | bytes 5767184 | tf_op jit(solution)/shard_map/all_gather | solution.py:174
  553.9 8.2 %fusion.72 = f32[512,1408]{1,0:T(8,128)} fusion(bf16[512,2048]{1,0:T(8,128)(2,1)} %multiply_convert_fusion, bf16[2048,1408]{1,0:T(8,128)(2,1)} %all-gather.19.cloned.1.call-done), kind=kOutput, calls=%fused_computation.131 | convolution fusion | flops 2952790016 | bytes 10747904 | tf_op jit(solution)/shard_map/dot_general | solution.py:172
  562.1 84.5 %all-gather.21.cloned.1.call-done = bf16[2048,1408]{1,0:T(8,128)(2,1)} async-done(((bf16[256,1408]{1,0:T(8,128)(2,1)}), bf16[2048,1408]{1,0:T(8,128)(2,1)}) %all-gather.21.cloned.1.call-update) | async-done | bytes 5767184 | tf_op jit(solution)/shard_map/all_gather | solution.py:179
  646.6 93.4 %all-gather.23.cloned.1.call-done = bf16[1408,2048]{1,0:T(8,128)(2,1)} async-done(((bf16[1408,256]{1,0:T(8,128)(2,1)}), bf16[1408,2048]{1,0:T(8,128)(2,1)}) %all-gather.23.cloned.1.call-update) | async-done | bytes 5767184 | tf_op jit(solution)/shard_map/all_gather | solution.py:182
  740.0 13.3 %convolution_convert_fusion = bf16[512,2048]{1,0:T(8,128)(2,1)} fusion(bf16[1408,2048]{1,0:T(8,128)(2,1)} %all-gather.23.cloned.1.call-done, bf16[512,2048]{1,0:T(8,128)(2,1)S(1)} %copy-done.3, bf16[2048,1408]{1,0:T(8,128)(2,1)} %all-gather.21.cloned.1.call-done, f32[512,1408]{1,0:T(8,128)} %fusion.72), kind=kOutput, calls=%fused_computation.79 | convolution fusion | flops 5910953984 | bytes 18612224 | tf_op jit(solution)/shard_map/dot_general | solution.py:185
  753.3 29.5 %reduce-scatter.2.cloned.1.call-done = bf16[128,2048]{1,0:T(8,128)(2,1)} async-done(((bf16[512,2048]{1,0:T(8,128)(2,1)}), bf16[128,2048]{1,0:T(8,128)(2,1)}) %reduce-scatter.2.cloned.1.call-update) | async-done | bytes 524304 | tf_op jit(solution)/shard_map/reduce_scatter | solution.py:184
  (376 shorter events, 180.5 us)
Async XLA Ops:
  6.5 396.8 %copy-start = (bf16[256,2048]{1,0:T(8,128)(2,1)S(1)}, bf16[256,2048]{1,0:T(8,128)(2,1)}, u32[]{:S(2)}) copy-start(bf16[256,2048]{1,0:T(8,128)(2,1)} %param.33) | copy-start | bytes 3145732
  6.5 67.3 %all-gather.11.cloned.1.call-start = ((), (), s32[]{:S(2)}) async-start(), calls=%async_computation.2 | async-start | bytes 2359296 | tf_op jit(solution)/shard_map/all_gather | solution.py:114
  7.3 141.4 %all-gather.15.cloned.1.call-start = ((), (), s32[]{:S(2)}) async-start(), calls=%async_computation.4 | async-start | bytes 4718592 | tf_op jit(solution)/shard_map/all_gather | solution.py:115
  8.0 190.5 %all-gather.13.cloned.1.call-start = ((), (), s32[]{:S(2)}) async-start(), calls=%async_computation.3 | async-start | bytes 2359296 | tf_op jit(solution)/shard_map/all_gather | solution.py:116
  9.8 238.4 %all-gather.17.cloned.1.call-start = ((), (), s32[]{:S(2)}) async-start(), calls=%async_computation.5 | async-start | bytes 2359296 | tf_op jit(solution)/shard_map/all_gather | solution.py:117
  11.5 399.0 %all-gather.9.cloned.1.call-start = ((), (), s32[]{:S(2)}) async-start(), calls=%async_computation.1 | async-start | bytes 2621440 | tf_op jit(solution)/shard_map/all_gather | solution.py:88
  12.2 9.3 %collective-permute-start.3 = (bf16[256,2,256]{0,2,1:T(8,128)(2,1)S(1)}, bf16[256,2,256]{0,2,1:T(8,128)(2,1)S(1)}, u32[]{:S(2)}, u32[]{:S(2)}) collective-permute-start(bf16[256,2,256]{0,2,1:T(8,128)(2,1)S(1)} %copy.82), channel_id=1, source_target_pairs={{0,4},{4,0},{8,12},{12,8},{16,20},{20,16},{24,28},{28,24},{1,5},{5... | collective-permute-start | bytes 786440 | tf_op jit(solution)/shard_map/ppermute | solution.py:16
  21.5 15.5 %collective-permute-start.4 = (bf16[256,2,256]{0,2,1:T(8,128)(2,1)S(1)}, bf16[256,2,256]{0,2,1:T(8,128)(2,1)S(1)}, u32[]{:S(2)}, u32[]{:S(2)}) collective-permute-start(bf16[256,2,256]{0,2,1:T(8,128)(2,1)S(1)} %collective-permute-done.3), channel_id=1, source_target_pairs={{0,8},{4,12},{8,0},{12,4},{16,24},{20,28},{24,16},{28,20},{1,9},{5... | collective-permute-start | bytes 786440 | tf_op jit(solution)/shard_map/ppermute | solution.py:16
  23.5 5.0 collective-permute-start
  28.5 12.9 %collective-permute-start.1 = (bf16[256,2,128]{2,1,0:T(2,128)(2,1)S(1)}, bf16[256,2,128]{2,1,0:T(2,128)(2,1)S(1)}, u32[]{:S(2)}, u32[]{:S(2)}) collective-permute-start(bf16[256,2,128]{2,1,0:T(2,128)(2,1)S(1)} %collective-permute-done), channel_id=1, source_target_pairs={{0,8},{4,12},{8,0},{12,4},{16,24},{20,28},{24,16},{28,20},{1,9},{5... | collective-permute-start | bytes 393224 | tf_op jit(solution)/shard_map/ppermute | solution.py:16
  37.0 35.9 %collective-permute-start.5 = (bf16[256,2,256]{0,2,1:T(8,128)(2,1)S(1)}, bf16[256,2,256]{0,2,1:T(8,128)(2,1)S(1)}, u32[]{:S(2)}, u32[]{:S(2)}) collective-permute-start(bf16[256,2,256]{0,2,1:T(8,128)(2,1)S(1)} %collective-permute-done.4), channel_id=1, source_target_pairs={{0,16},{4,20},{8,24},{12,28},{16,0},{20,4},{24,8},{28,12},{1,17},{... | collective-permute-start | bytes 786440 | tf_op jit(solution)/shard_map/ppermute | solution.py:16
  41.5 31.3 %collective-permute-start.2 = (bf16[256,2,128]{2,1,0:T(2,128)(2,1)S(1)}, bf16[256,2,128]{2,1,0:T(2,128)(2,1)S(1)}, u32[]{:S(2)}, u32[]{:S(2)}) collective-permute-start(bf16[256,2,128]{2,1,0:T(2,128)(2,1)S(1)} %collective-permute-done.1), channel_id=1, source_target_pairs={{0,16},{4,20},{8,24},{12,28},{16,0},{20,4},{24,8},{28,12},{1,17},{... | collective-permute-start | bytes 393224 | tf_op jit(solution)/shard_map/ppermute | solution.py:16
  43.0 416.3 %all-reduce.2.cloned.1.call-start = ((), (), s32[]{:S(2)}) async-start(), calls=%async_computation.6 | async-start | bytes 4194304 | tf_op jit(solution)/shard_map/psum | solution.py:161
  384.5 5.0 collective-permute-start.9
  385.1 6.5 collective-permute-start.6
  389.6 5.1 collective-permute-start.10
  391.6 6.7 collective-permute-start.7
  394.7 8.6 %collective-permute-start.11 = (bf16[256,256]{0,1:T(8,128)(2,1)S(1)}, bf16[256,256]{0,1:T(8,128)(2,1)S(1)}, u32[]{:S(2)}, u32[]{:S(2)}) collective-permute-start(bf16[256,256]{0,1:T(8,128)(2,1)S(1)} %collective-permute-done.10), channel_id=1, source_target_pairs={{0,16},{4,20},{8,24},{12,28},{16,0},{20,4},{24,8},{28,12},{1,17},{... | collective-permute-start | bytes 393224 | tf_op jit(solution)/shard_map/ppermute | solution.py:16
  398.3 7.9 collective-permute-start.8
  408.3 145.6 %all-gather.19.cloned.1.call-start = ((), (), s32[]{:S(2)}) async-start(), calls=%async_computation.7 | async-start | bytes 6488064 | tf_op jit(solution)/shard_map/all_gather | solution.py:174
  409.0 237.6 %all-gather.21.cloned.1.call-start = ((), (), s32[]{:S(2)}) async-start(), calls=%async_computation.8 | async-start | bytes 6488064 | tf_op jit(solution)/shard_map/all_gather | solution.py:179
  409.8 330.2 %all-gather.23.cloned.1.call-start = ((), (), s32[]{:S(2)}) async-start(), calls=%async_computation.9 | async-start | bytes 6488064 | tf_op jit(solution)/shard_map/all_gather | solution.py:182
  410.5 372.3 %reduce-scatter.2.cloned.1.call-start = ((), (), s32[]{:S(2)}) async-start(), calls=%async_computation.10 | async-start | bytes 2621440 | tf_op jit(solution)/shard_map/reduce_scatter | solution.py:184
  465.9 274.1 %copy-start.3 = (bf16[512,2048]{1,0:T(8,128)(2,1)S(1)}, bf16[512,2048]{1,0:T(8,128)(2,1)}, u32[]{:S(2)}) copy-start(bf16[512,2048]{1,0:T(8,128)(2,1)} %multiply_convert_fusion) | copy-start | bytes 6291460
  (49 other events, 137.6 us)
Sparse Core Ops, SparseCore 0:
  9.5 64.2 all-gather.10
  75.9 72.7 all-gather.14
  150.9 47.5 all-gather.12
  200.6 47.5 all-gather.16
  249.6 21.0 all-gather.8
  408.4 50.8 all-reduce.1
  461.5 92.3 all-gather.18
  556.1 90.4 all-gather.20
  648.7 91.2 all-gather.22
  753.4 29.3 reduce-scatter.1
where the time goes:
time: 794 us; the launch traced here: 792 us
  waiting for transfers between devices  548 us (69%)
  local copies, waits for them, and re-layouts  102 us (13%)
  matrix products  52.3 us (7%)
  loops' own time  26.4 us (3%)
  other arithmetic  25.5 us (3%)
  starting transfers between devices  23.7 us (3%)
  between operations  13.9 us (2%)
    all_gather x1, waiting for transfers between devices, per_device(): down_full = lax.all_gather(down_weight, 'sp', axis=1, tiled=True)  93.4 us
    all_gather x1, waiting for transfers between devices, per_device(): lax.all_gather(gate_weight, 'sp', axis=0, tiled=True)  88 us
    all_gather x1, waiting for transfers between devices, per_device(): lax.all_gather(up_weight, 'sp', axis=0, tiled=True)  84.5 us
    ppermute x12, waiting for transfers between devices, from_partner(): return lax.ppermute(value, axis, pairs)  57.4 us
    all_gather x1, waiting for transfers between devices, per_device(): keys_second = lax.all_gather(key_large, 'sp', axis=0, tiled=True)  54.6 us
    all_gather x1, waiting for transfers between devices, per_device(): values_second = lax.all_gather(value_large, 'sp', axis=0, tiled=True)  49.7 us
    psum x1, waiting for transfers between devices, per_device(): lax.psum((jnp.dot(attended_small, output_small, preferred_element_type=jn...  48.7 us
    all_gather x1, waiting for transfers between devices, per_device(): values_first = lax.all_gather(value_small, 'sp', axis=0, tiled=True)  38.1 us
  transfers between devices with their start and end apart: 22, of which 18 were waited for; matrix products, arithmetic and copies ran while one was open for 20% of the time, Pallas kernels for 0%

commit v1 on v0

--- a/solution.py
+++ b/solution.py
@@ -176,7 +176,9 @@
     )
     up_rows = jnp.dot(
         whole_rows,
-        lax.all_gather(up_weight, "sp", axis=0, tiled=True),
+        jnp.concatenate(
+            lax.all_to_all(jnp.stack([up_weight] * lax.axis_size("sp")), "sp", 0, 0), axis=0
+        ),
         preferred_element_type=jnp.float32,
     )
     down_full = lax.all_gather(down_weight, "sp", axis=1, tiled=True)

time: 794 us -> 758 us (0.955)
  waiting for transfers between devices: 548 us -> 504 us
    all_gather x1 -> x0, waiting for transfers between devices: 84.5 us -> none  [per_device(): lax.all_gather(up_weight, 'sp', axis=0, tiled=True)]
    all_gather x1, waiting for transfers between devices: 88 us -> 142 us  [per_device(): lax.all_gather(gate_weight, 'sp', axis=0, tiled=True)]
  transfers between devices with their start and end apart: 22 -> 22, of which waited for: 18 -> 17; matrix products, arithmetic and copies ran while one was open for 20% -> 21% of each run, Pallas kernels for 0% -> 0%
where the time goes in v1:
time: 758 us; the launch traced here: 755 us
  waiting for transfers between devices  504 us (66%)
  local copies, waits for them, and re-layouts  105 us (14%)
  matrix products  52.4 us (7%)
  loops' own time  27.8 us (4%)
  starting transfers between devices  27 us (4%)
  other arithmetic  25.5 us (3%)
  between operations  13.6 us (2%)
    all_gather x1, waiting for transfers between devices, per_device(): lax.all_gather(gate_weight, 'sp', axis=0, tiled=True)  142 us
    all_gather x1, waiting for transfers between devices, per_device(): down_full = lax.all_gather(down_weight, 'sp', axis=1, tiled=True)  85.8 us
    ppermute x12, waiting for transfers between devices, from_partner(): return lax.ppermute(value, axis, pairs)  58.9 us
    all_gather x1, waiting for transfers between devices, per_device(): keys_second = lax.all_gather(key_large, 'sp', axis=0, tiled=True)  54.6 us
    all_gather x1, waiting for transfers between devices, per_device(): values_second = lax.all_gather(value_large, 'sp', axis=0, tiled=True)  49.7 us
    psum x1, waiting for transfers between devices, per_device(): lax.psum((jnp.dot(attended_small, output_small, preferred_element_type=jn...  41.2 us
    all_gather x1, waiting for transfers between devices, per_device(): values_first = lax.all_gather(value_small, 'sp', axis=0, tiled=True)  38.1 us
    reduce_scatter x1, waiting for transfers between devices, per_device(): lax.psum_scatter(jnp.dot(hidden, down_full, preferred_element_type=jnp.fl...  29.5 us
  transfers between devices with their start and end apart: 22, of which 17 were waited for; matrix products, arithmetic and copies ran while one was open for 21% of the time, Pallas kernels for 0%

profile of v1, /device:TPU:0, one launch (start us, length us, event | category | flops | bytes accessed | tf_op | source)
XLA Modules:
  0.0 755.3 jit_solution(9991061391355939896)
XLA Ops:
  15.2 6.3 collective-permute-done.3
  30.0 7.0 collective-permute-done.4
  43.6 29.2 %collective-permute-done.2 = bf16[256,2,128]{2,1,0:T(2,128)(2,1)S(1)} collective-permute-done((bf16[256,2,128]{2,1,0:T(2,128)(2,1)S(1)}, bf16[256,2,128]{2,1,0:T(2,128)(2,1)S(1)}, u32[]{:S(2)}, u32[]{:S(2)}) %collective-permute-start.2) | collective-permute-done | bytes 131104 | tf_op jit(solution)/shard_map/ppermute | solution.py:16
  73.8 9.7 %reshape.132 = bf16[8,512,2,2,64]{4,3,2,1,0:T(2,128)(2,1)} reshape(bf16[4096,2,128]{2,1,0:T(2,128)(2,1)} %all-gather.10.cloned.1.call-done) | data formatting | bytes 4194304 | tf_op jit(solution)/shard_map/reshape | solution.py:122
  83.5 10.6 %copy.56 = bf16[8,512,2,2,64]{1,4,3,2,0:T(8,128)(2,1)} copy(bf16[8,512,2,2,64]{4,3,2,1,0:T(2,128)(2,1)} %reshape.132) | data formatting | bytes 4194304 | tf_op jit(solution)/shard_map/while | solution.py:149
  94.1 54.6 %all-gather.14.cloned.1.call-done = bf16[4096,2,256]{2,1,0:T(2,128)(2,1)} async-done(((bf16[512,2,256]{2,1,0:T(2,128)(2,1)}), bf16[4096,2,256]{2,1,0:T(2,128)(2,1)}) %all-gather.14.cloned.1.call-update) | async-done | bytes 4194320 | tf_op jit(solution)/shard_map/all_gather | solution.py:115
  148.7 11.7 %reshape.133 = bf16[8,512,2,2,128]{4,3,2,1,0:T(2,128)(2,1)} reshape(bf16[4096,2,256]{2,1,0:T(2,128)(2,1)} %all-gather.14.cloned.1.call-done) | data formatting | bytes 8388608 | tf_op jit(solution)/shard_map/reshape | solution.py:123
  160.4 38.1 %all-gather.12.cloned.1.call-done = bf16[4096,2,128]{2,0,1:T(8,128)(2,1)} async-done(((bf16[512,2,128]{2,0,1:T(8,128)(2,1)}), bf16[4096,2,128]{2,0,1:T(8,128)(2,1)}) %all-gather.12.cloned.1.call-update) | async-done | bytes 2097168 | tf_op jit(solution)/shard_map/all_gather | solution.py:116
  198.5 49.7 %all-gather.16.cloned.1.call-done = bf16[4096,2,128]{2,0,1:T(8,128)(2,1)} async-done(((bf16[512,2,128]{2,0,1:T(8,128)(2,1)}), bf16[4096,2,128]{2,0,1:T(8,128)(2,1)}) %all-gather.16.cloned.1.call-update) | async-done | bytes 2097168 | tf_op jit(solution)/shard_map/all_gather | solution.py:117
  251.6 126.6 %while.32 = (s32[]{:T(128)}, f32[2,2,256]{2,1,0:T(2,128)S(1)}, f32[2,2,256]{2,1,0:T(2,128)S(1)}, f32[2,2,256,128]{3,2,1,0:T(8,128)}, f32[2,2,256]{2,1,0:T(2,128)...) while((s32[]{:T(128)}, f32[2,2,256]{2,1,0:T(2,128)S(1)}, ...), condition=%wide.region_13.14_spmd, body=%wide.region_0.13_spmd.sunk | while | flops 968106496 | bytes 58991568 | solution.py:149
  259.0 5.8 conditional.5
  279.8 5.8 conditional.5
  294.8 5.8 conditional.5
  309.9 5.8 conditional.5
  325.0 5.8 conditional.5
  340.1 5.8 conditional.5
  355.1 5.8 conditional.5
  370.2 5.8 conditional.5
  419.8 41.2 %all-reduce.2.cloned.1.call-done = bf16[512,2048]{1,0:T(8,128)(2,1)} async-done(((bf16[512,2048]{1,0:T(8,128)(2,1)}), bf16[512,2048]{1,0:T(8,128)(2,1)}) %all-reduce.2.cloned.1.call-update) | async-done | bytes 2097168 | tf_op jit(solution)/shard_map/psum | solution.py:161
  467.5 142.3 %all-gather.18.cloned.1.call-done = bf16[2048,1408]{1,0:T(8,128)(2,1)} async-done(((bf16[256,1408]{1,0:T(8,128)(2,1)}), bf16[2048,1408]{1,0:T(8,128)(2,1)}) %all-gather.18.cloned.1.call-update) | async-done | bytes 5767184 | tf_op jit(solution)/shard_map/all_gather | solution.py:174
  609.8 8.3 %fusion.72 = f32[512,1408]{1,0:T(8,128)} fusion(bf16[512,2048]{1,0:T(8,128)(2,1)} %multiply_convert_fusion, bf16[2048,1408]{1,0:T(8,128)(2,1)} %all-gather.18.cloned.1.call-done), kind=kOutput, calls=%fused_computation.131 | convolution fusion | flops 2952790016 | bytes 10747904 | tf_op jit(solution)/shard_map/dot_general | solution.py:172
  618.1 85.8 %all-gather.20.cloned.1.call-done = bf16[1408,2048]{1,0:T(8,128)(2,1)} async-done(((bf16[1408,256]{1,0:T(8,128)(2,1)}), bf16[1408,2048]{1,0:T(8,128)(2,1)}) %all-gather.20.cloned.1.call-update) | async-done | bytes 5767184 | tf_op jit(solution)/shard_map/all_gather | solution.py:184
  703.9 13.3 %convolution_convert_fusion = bf16[512,2048]{1,0:T(8,128)(2,1)} fusion(bf16[1408,2048]{1,0:T(8,128)(2,1)} %all-gather.20.cloned.1.call-done, bf16[512,2048]{1,0:T(8,128)(2,1)S(1)} %copy-done.3, bf16[2048,1408]{1,0:T(8,128)(2,1)} %bitcast.37, f32[512,1408]{1,0:T(8,128)} %fusion.72), kind=kOutput, calls=%fused_computation.79 | convolution fusion | flops 5910953984 | bytes 18612224 | tf_op jit(solution)/shard_map/dot_general | solution.py:187
  717.2 29.5 %reduce-scatter.2.cloned.1.call-done = bf16[128,2048]{1,0:T(8,128)(2,1)} async-done(((bf16[512,2048]{1,0:T(8,128)(2,1)}), bf16[128,2048]{1,0:T(8,128)(2,1)}) %reduce-scatter.2.cloned.1.call-update) | async-done | bytes 524304 | tf_op jit(solution)/shard_map/reduce_scatter | solution.py:186
  (378 shorter events, 182.6 us)
Async XLA Ops:
  6.5 398.8 %copy-start = (bf16[256,2048]{1,0:T(8,128)(2,1)S(1)}, bf16[256,2048]{1,0:T(8,128)(2,1)}, u32[]{:S(2)}) copy-start(bf16[256,2048]{1,0:T(8,128)(2,1)} %param.33) | copy-start | bytes 3145732
  6.5 67.3 %all-gather.10.cloned.1.call-start = ((), (), s32[]{:S(2)}) async-start(), calls=%async_computation.3 | async-start | bytes 2359296 | tf_op jit(solution)/shard_map/all_gather | solution.py:114
  7.3 141.4 %all-gather.14.cloned.1.call-start = ((), (), s32[]{:S(2)}) async-start(), calls=%async_computation.5 | async-start | bytes 4718592 | tf_op jit(solution)/shard_map/all_gather | solution.py:115
  8.0 190.5 %all-gather.12.cloned.1.call-start = ((), (), s32[]{:S(2)}) async-start(), calls=%async_computation.4 | async-start | bytes 2359296 | tf_op jit(solution)/shard_map/all_gather | solution.py:116
  9.8 238.4 %all-gather.16.cloned.1.call-start = ((), (), s32[]{:S(2)}) async-start(), calls=%async_computation.6 | async-start | bytes 2359296 | tf_op jit(solution)/shard_map/all_gather | solution.py:117
  11.5 408.3 %all-gather.8.cloned.1.call-start = ((), (), s32[]{:S(2)}) async-start(), calls=%async_computation.2 | async-start | bytes 2621440 | tf_op jit(solution)/shard_map/all_gather | solution.py:88
  12.2 9.3 %collective-permute-start.3 = (bf16[256,2,256]{0,2,1:T(8,128)(2,1)S(1)}, bf16[256,2,256]{0,2,1:T(8,128)(2,1)S(1)}, u32[]{:S(2)}, u32[]{:S(2)}) collective-permute-start(bf16[256,2,256]{0,2,1:T(8,128)(2,1)S(1)} %copy.82), channel_id=1, source_target_pairs={{0,4},{4,0},{8,12},{12,8},{16,20},{20,16},{24,28},{28,24},{1,5},{5... | collective-permute-start | bytes 786440 | tf_op jit(solution)/shard_map/ppermute | solution.py:16
  21.5 15.5 %collective-permute-start.4 = (bf16[256,2,256]{0,2,1:T(8,128)(2,1)S(1)}, bf16[256,2,256]{0,2,1:T(8,128)(2,1)S(1)}, u32[]{:S(2)}, u32[]{:S(2)}) collective-permute-start(bf16[256,2,256]{0,2,1:T(8,128)(2,1)S(1)} %collective-permute-done.3), channel_id=1, source_target_pairs={{0,8},{4,12},{8,0},{12,4},{16,24},{20,28},{24,16},{28,20},{1,9},{5... | collective-permute-start | bytes 786440 | tf_op jit(solution)/shard_map/ppermute | solution.py:16
  23.5 5.0 collective-permute-start
  28.5 12.9 %collective-permute-start.1 = (bf16[256,2,128]{2,1,0:T(2,128)(2,1)S(1)}, bf16[256,2,128]{2,1,0:T(2,128)(2,1)S(1)}, u32[]{:S(2)}, u32[]{:S(2)}) collective-permute-start(bf16[256,2,128]{2,1,0:T(2,128)(2,1)S(1)} %collective-permute-done), channel_id=1, source_target_pairs={{0,8},{4,12},{8,0},{12,4},{16,24},{20,28},{24,16},{28,20},{1,9},{5... | collective-permute-start | bytes 393224 | tf_op jit(solution)/shard_map/ppermute | solution.py:16
  37.0 35.9 %collective-permute-start.5 = (bf16[256,2,256]{0,2,1:T(8,128)(2,1)S(1)}, bf16[256,2,256]{0,2,1:T(8,128)(2,1)S(1)}, u32[]{:S(2)}, u32[]{:S(2)}) collective-permute-start(bf16[256,2,256]{0,2,1:T(8,128)(2,1)S(1)} %collective-permute-done.4), channel_id=1, source_target_pairs={{0,16},{4,20},{8,24},{12,28},{16,0},{20,4},{24,8},{28,12},{1,17},{... | collective-permute-start | bytes 786440 | tf_op jit(solution)/shard_map/ppermute | solution.py:16
  41.5 31.3 %collective-permute-start.2 = (bf16[256,2,128]{2,1,0:T(2,128)(2,1)S(1)}, bf16[256,2,128]{2,1,0:T(2,128)(2,1)S(1)}, u32[]{:S(2)}, u32[]{:S(2)}) collective-permute-start(bf16[256,2,128]{2,1,0:T(2,128)(2,1)S(1)} %collective-permute-done.1), channel_id=1, source_target_pairs={{0,16},{4,20},{8,24},{12,28},{16,0},{20,4},{24,8},{28,12},{1,17},{... | collective-permute-start | bytes 393224 | tf_op jit(solution)/shard_map/ppermute | solution.py:16
  43.0 418.0 %all-reduce.2.cloned.1.call-start = ((), (), s32[]{:S(2)}) async-start(), calls=%async_computation.7 | async-start | bytes 4194304 | tf_op jit(solution)/shard_map/psum | solution.py:161
  386.4 5.0 collective-permute-start.9
  386.9 6.5 collective-permute-start.6
  391.4 6.2 collective-permute-start.10
  393.4 6.6 collective-permute-start.7
  397.6 7.7 %collective-permute-start.11 = (bf16[256,256]{0,1:T(8,128)(2,1)S(1)}, bf16[256,256]{0,1:T(8,128)(2,1)S(1)}, u32[]{:S(2)}, u32[]{:S(2)}) collective-permute-start(bf16[256,256]{0,1:T(8,128)(2,1)S(1)} %collective-permute-done.10), channel_id=1, source_target_pairs={{0,16},{4,20},{8,24},{12,28},{16,0},{20,4},{24,8},{28,12},{1,17},{... | collective-permute-start | bytes 393224 | tf_op jit(solution)/shard_map/ppermute | solution.py:16
  399.9 8.2 %collective-permute-start.8 = (bf16[256,256]{0,1:T(8,128)(2,1)S(1)}, bf16[256,256]{0,1:T(8,128)(2,1)S(1)}, u32[]{:S(2)}, u32[]{:S(2)}) collective-permute-start(bf16[256,256]{0,1:T(8,128)(2,1)S(1)} %collective-permute-done.7), channel_id=1, source_target_pairs={{0,16},{4,20},{8,24},{12,28},{16,0},{20,4},{24,8},{28,12},{1,17},{... | collective-permute-start | bytes 393224 | tf_op jit(solution)/shard_map/ppermute | solution.py:16
  410.3 199.5 %all-gather.18.cloned.1.call-start = ((), (), s32[]{:S(2)}) async-start(), calls=%async_computation.8 | async-start | bytes 6488064 | tf_op jit(solution)/shard_map/all_gather | solution.py:174
  414.3 203.8 %all-to-all-start = ((bf16[8,256,1408]{2,1,0:T(8,128)(2,1)}), bf16[8,256,1408]{2,1,0:T(8,128)(2,1)}, u32[]{:S(2)}, u32[]{:S(2)}) async-start(bf16[8,256,1408]{2,1,0:T(8,128)(2,1)} %stack.2), calls=%async_computation | async-start | bytes 11534336 | tf_op jit(solution)/shard_map/all_to_all | solution.py:180
  419.0 284.9 %all-gather.20.cloned.1.call-start = ((), (), s32[]{:S(2)}) async-start(), calls=%async_computation.9 | async-start | bytes 6488064 | tf_op jit(solution)/shard_map/all_gather | solution.py:184
  419.8 327.0 %reduce-scatter.2.cloned.1.call-start = ((), (), s32[]{:S(2)}) async-start(), calls=%async_computation.10 | async-start | bytes 2621440 | tf_op jit(solution)/shard_map/reduce_scatter | solution.py:186
  467.5 236.4 %copy-start.3 = (bf16[512,2048]{1,0:T(8,128)(2,1)S(1)}, bf16[512,2048]{1,0:T(8,128)(2,1)}, u32[]{:S(2)}) copy-start(bf16[512,2048]{1,0:T(8,128)(2,1)} %multiply_convert_fusion) | copy-start | bytes 6291460
  (50 other events, 131.3 us)
Sparse Core Ops, SparseCore 0:
  9.5 64.2 all-gather.9
  75.9 72.7 all-gather.13
  150.9 47.5 all-gather.11
  200.6 47.5 all-gather.15
  249.6 21.0 all-gather.7
  410.4 50.5 all-reduce.1
  463.2 146.5 all-gather.17
  611.8 92.0 all-gather.19
  717.3 29.3 reduce-scatter.1
